TPU v7x, 32 devices: a whole 2x2x4 slice. The times are simulated.
32 devices in a mesh: sp: 4 (over z), fs: 4 (over y, x), tp: 2 (over core).
Axes of the slice: x: 2, y: 2, z: 4, core: 2. Of those that a mesh axis runs over, the one named last changes fastest.
Arguments:
- tokens: bfloat16 [4, 2048, 2048], P('fs', ('sp', 'tp')), may hold values from -6 to 6
- norm_gain: float32 [2048], replicated, may hold values from 0.1 to 1.9
- query_weight: bfloat16 [2048, 1024], P('sp', 'tp'), may hold values from -20 to 20
- key_matrix: bfloat16 [2048, 256], P('sp', 'tp'), may hold values from -0.125 to 0.125
- value_matrix: bfloat16 [2048, 256], P('sp', 'tp'), may hold values from -0.125 to 0.125
- pool_in_weight: bfloat16 [2048, 1024], P('sp', 'tp'), may hold values from -0.125 to 0.125
- head_sink_logit: float32 [16], replicated, may hold values from 2 to 6
- pool_mix: bfloat16 [4, 256, 256], replicated, may hold values from -0.375 to 0.375
- pool_gain: float32 [1024], replicated, may hold values from 0.1 to 1.9
- attn_out_weight: bfloat16 [1024, 2048], P('tp', 'sp'), may hold values from -1 to 1
- pool_out_weight: bfloat16 [1024, 2048], P('tp', 'sp'), may hold values from -0.125 to 0.125
Outputs:
- mixed: bfloat16 [4, 2048, 2048], P('fs', ('sp', 'tp'))
- row_log_weight_sum: float32 [4, 16, 2048], P('fs', 'tp', 'sp')
All inputs are finite; a program needn't handle non-finite values.
Results may differ from a plain program's by a relative error of at most 0.0095.
The roundings to bfloat16 on the way count: a program that leaves them out, or rounds other values in their place, can miss the bound.
Values may be sent and summed in bfloat16 or wider, within the bound.
No kernel may reach another device: no remote copies, remote signals or barrier semaphores. Data moves between devices by JAX's collectives and lax.ppermute only.
A program may use at most 64 MiB of HBM per device.

v0:
```python
import jax
import jax.numpy as jnp
from jax import lax
from jax.sharding import PartitionSpec as P

HEAD_SIZE = 64
WINDOW = 128
POOL_CH = 256
EPSILON = 1e-06
POOL_SPANS = (2, 4, 8, 16)


def passed_along(shard, axis, by):
    size = lax.axis_size(axis)
    pairs = [(i, i + by) for i in range(size) if 0 <= i + by < size]
    return lax.ppermute(shard, axis, pairs)


def windowed_attend(
    query_rows, key_rows, value_rows, key_tail, value_tail, sinks, kv_heads, group, first_pos
):
    rows = query_rows.shape[0]
    blocks = rows // WINDOW
    width = key_rows.shape[1]
    ext_keys = jnp.concatenate([key_tail, key_rows], 0)
    ext_values = jnp.concatenate([value_tail, value_rows], 0)

    def banded(table):
        return jnp.concatenate(
            [
                table[:rows].reshape(blocks, WINDOW, width),
                table[WINDOW:].reshape(blocks, WINDOW, width),
            ],
            axis=1,
        )

    band_keys = banded(ext_keys).reshape(blocks, 2 * WINDOW, kv_heads, HEAD_SIZE)
    band_values = banded(ext_values).reshape(blocks, 2 * WINDOW, kv_heads, HEAD_SIZE)
    query_blocks = query_rows.reshape(blocks, WINDOW, kv_heads, group, HEAD_SIZE)
    scores = jnp.einsum(
        "bqkgd,bskd->bkgqs", query_blocks, band_keys, preferred_element_type=jnp.float32
    ) * HEAD_SIZE ** (-0.5)
    query_pos = first_pos + jnp.arange(rows).reshape(blocks, WINDOW, 1)
    key_pos = (
        first_pos
        - WINDOW
        + jnp.arange(blocks).reshape(blocks, 1, 1) * WINDOW
        + jnp.arange(2 * WINDOW).reshape(1, 1, 2 * WINDOW)
    )
    offset = query_pos - key_pos
    allowed = (offset >= 0) & (offset < WINDOW) & (key_pos >= 0)
    scores = jnp.where(allowed[:, None, None], scores, -jnp.inf)
    sink_grid = sinks.reshape(1, kv_heads, group, 1, 1)
    top = jnp.maximum(jnp.max(scores, axis=-1, keepdims=True), sink_grid)
    weights = jnp.exp(scores - top)
    total = jnp.sum(weights, axis=-1, keepdims=True) + jnp.exp(sink_grid - top)
    probs = (weights / total).astype(jnp.bfloat16)
    mixed = jnp.einsum(
        "bkgqs,bskd->bqkgd", probs, band_values, preferred_element_type=jnp.float32
    ).astype(jnp.bfloat16)
    row_log_weight_sum = (top + jnp.log(total))[..., 0]
    return (
        mixed.reshape(rows, kv_heads * group * HEAD_SIZE),
        row_log_weight_sum.transpose(1, 2, 0, 3).reshape(kv_heads * group, rows),
    )


def pool_branch(pool_rows, pool_tail, mixing, scales, group_start, first_pos):
    rows = pool_rows.shape[0]
    columns = pool_rows.shape[1]
    pool_reach = max(POOL_SPANS)
    extended = jnp.concatenate([pool_tail, pool_rows], 0).astype(jnp.float32)
    group_index = group_start + jnp.arange(columns) // POOL_CH
    span_table = jnp.array(POOL_SPANS, jnp.int32)
    matches = group_index[:, None] == jnp.arange(len(POOL_SPANS))[None, :]
    span_of_col = jnp.sum(jnp.where(matches, span_table[None, :], 0), axis=1)
    trailing = jnp.zeros((rows, columns), jnp.float32)
    for lag in range(pool_reach):
        trailing = trailing + jnp.where(
            lag < span_of_col[None, :], extended[pool_reach - lag : pool_reach - lag + rows], 0.0
        )
    position = first_pos + jnp.arange(rows)
    count = jnp.minimum(position[:, None] + 1, span_of_col[None, :]).astype(jnp.float32)
    centred = (trailing / count - extended[pool_reach:]).astype(jnp.bfloat16)
    grouped = centred.reshape(rows, columns // POOL_CH, POOL_CH)
    product = jnp.einsum(
        "rgc,gcd->rgd", grouped, mixing, preferred_element_type=jnp.float32
    ).reshape(rows, columns)
    return (product * scales).astype(jnp.bfloat16)


def local(
    tokens,
    norm_gain,
    query_weight,
    key_matrix,
    value_matrix,
    pool_in_weight,
    head_sink_logit,
    pool_mix,
    pool_gain,
    attn_out_weight,
    pool_out_weight,
):
    tp_index = lax.axis_index("tp")
    sp_index = lax.axis_index("sp")
    q_cols = query_weight.shape[1]
    kv_cols = key_matrix.shape[1]
    pool_cols = pool_in_weight.shape[1]
    q_heads = q_cols // HEAD_SIZE
    kv_heads = kv_cols // HEAD_SIZE
    groups_dev = pool_cols // POOL_CH
    full_query, full_key, full_value, full_pool = (
        lax.all_gather(query_weight, "sp", axis=0, tiled=True),
        lax.all_gather(key_matrix, "sp", axis=0, tiled=True),
        lax.all_gather(value_matrix, "sp", axis=0, tiled=True),
        lax.all_gather(pool_in_weight, "sp", axis=0, tiled=True),
    )
    values_f = lax.all_gather(tokens[0], "tp", axis=0, tiled=True).astype(jnp.float32)
    scale = lax.rsqrt(jnp.mean(values_f * values_f, axis=-1, keepdims=True) + EPSILON)
    normed = (values_f * scale * norm_gain).astype(jnp.bfloat16)
    outputs = [
        jnp.dot(normed, weight, preferred_element_type=jnp.float32).astype(jnp.bfloat16)
        for weight in (full_query, full_key, full_value, full_pool)
    ]
    projected = jnp.concatenate(outputs, axis=1)
    rows = projected.shape[0]
    first_pos = sp_index * rows
    query_rows = projected[:, :q_cols]
    key_rows = projected[:, q_cols : q_cols + kv_cols]
    value_rows = projected[:, q_cols + kv_cols : q_cols + 2 * kv_cols]
    pool_rows = projected[:, q_cols + 2 * kv_cols :]
    pool_reach = max(POOL_SPANS)
    sinks = lax.dynamic_slice_in_dim(head_sink_logit, tp_index * q_heads, q_heads, 0)
    mixing = lax.dynamic_slice_in_dim(pool_mix, tp_index * groups_dev, groups_dev, 0)
    scales = lax.dynamic_slice_in_dim(pool_gain, tp_index * pool_cols, pool_cols, 0)
    key_tail, value_tail, pool_tail = passed_along(
        (key_rows[rows - WINDOW :], value_rows[rows - WINDOW :], pool_rows[rows - pool_reach :]),
        "sp",
        1,
    )
    attn_part, log_part = windowed_attend(
        query_rows,
        key_rows,
        value_rows,
        key_tail,
        value_tail,
        sinks,
        kv_heads,
        q_heads // kv_heads,
        first_pos,
    )
    pool_part = pool_branch(pool_rows, pool_tail, mixing, scales, tp_index * groups_dev, first_pos)
    half_attn, half_pool = (
        lax.all_gather(attn_out_weight, "sp", axis=1, tiled=True),
        lax.all_gather(pool_out_weight, "sp", axis=1, tiled=True),
    )
    result = lax.psum_scatter(
        jnp.dot(attn_part, half_attn, preferred_element_type=jnp.float32)
        + jnp.dot(pool_part, half_pool, preferred_element_type=jnp.float32),
        "tp",
        scatter_dimension=0,
        tiled=True,
    ).astype(jnp.bfloat16)
    return (result[None], log_part[None])


def solution(mesh):
    in_specs = (
        P("fs", ("sp", "tp"), None),
        P(),
        P("sp", "tp"),
        P("sp", "tp"),
        P("sp", "tp"),
        P("sp", "tp"),
        P(),
        P(),
        P(),
        P("tp", "sp"),
        P("tp", "sp"),
    )
    out_specs = (P("fs", ("sp", "tp"), None), P("fs", "tp", "sp"))
    return jax.shard_map(local, mesh=mesh, in_specs=in_specs, out_specs=out_specs, check_vma=False)
```

profile of v0, /device:TPU:0, one launch (start us, length us, event | category | flops | bytes accessed | tf_op | source)
XLA Modules:
  0.0 243.1 jit_solution(15689682092924149541)
XLA Ops:
  7.2 0.0 all-gather.15.cloned.1.call-start
  7.3 0.7 all-gather.15.cloned.1.call-update
  7.9 0.0 all-gather.7.cloned.1.call-start
  8.0 0.7 all-gather.7.cloned.1.call-update
  8.7 0.0 all-gather.11.cloned.1.call-start
  8.7 0.7 all-gather.11.cloned.1.call-update
  9.4 0.0 all-gather.9.cloned.1.call-start
  9.5 0.5 all-gather.9.cloned.1.call-update
  10.0 0.0 all-gather.13.cloned.1.call-start
  10.1 0.5 all-gather.13.cloned.1.call-update
  10.6 0.0 reduce-scatter.2.cloned.1.call-start
  10.7 0.1 iota_add_fusion
  10.7 0.1 broadcast_compare_fusion
  10.8 17.6 %all_gather.23 = bf16[2048,128]{1,0:T(8,128)(2,1)S(1)} all-gather(bf16[512,128]{1,0:T(8,128)(2,1)} %param.15), channel_id=1, replica_groups=mesh['sp'=4,'fs'=4,'tp'=2] {'sp'}, dimensions={0}, use_global_device_ids=true | all-gather | bytes 655360 | tf_op jit(solution)/shard_map/all_gather | solution.py:115
  28.4 0.7 dynamic_slice.9
  29.1 0.1 max.26
  29.2 23.4 %all_gather.22 = bf16[2048,128]{1,0:T(8,128)(2,1)} all-gather(bf16[512,128]{1,0:T(8,128)(2,1)} %param.16), channel_id=1, replica_groups=mesh['sp'=4,'fs'=4,'tp'=2] {'sp'}, dimensions={0}, use_global_device_ids=true | all-gather | bytes 655360 | tf_op jit(solution)/shard_map/all_gather | solution.py:116
  52.6 0.1 select_reduce_fusion
  52.7 0.6 broadcast_compare_fusion.15
  53.4 0.1 dynamic_slice.11
  53.5 0.3 fusion.36
  53.8 0.0 all-gather.15.cloned.1.call-done
  53.9 2.2 fusion
  56.1 2.4 convolution_convert_fusion.2
  58.5 0.6 slice.86
  59.1 3.5 %collective-permute-start.1 = (bf16[128,128]{1,0:T(8,128)(2,1)}, bf16[128,128]{1,0:T(8,128)(2,1)}, u32[]{:S(2)}, u32[]{:S(2)}) collective-permute-start(bf16[128,128]{1,0:T(8,128)(2,1)} %slice.86), channel_id=1, source_target_pairs={{0,8},{8,16},{16,24},{1,9},{9,17},{17,25},{2,10},{10,18},{18,26},{... | collective-permute-start | bytes 98312 | tf_op jit(solution)/shard_map/ppermute | solution.py:16
  62.6 1.5 convolution_convert_fusion.3
  64.1 0.1 reshape.235
  64.2 0.6 slice.85
  64.8 0.1 reshape.233
  65.0 0.8 copy.45
  65.8 2.0 collective-permute-start
  67.8 0.8 copy.41
  68.5 0.8 pad_maximum_fusion
  69.3 0.1 reshape.234
  69.5 0.8 copy.44
  70.3 0.1 collective-permute-done
  70.3 0.1 reshape.232
  70.5 0.8 copy.40
  71.3 5.5 %all-gather.7.cloned.1.call-done = bf16[2048,512]{1,0:T(8,128)(2,1)} async-done(((bf16[512,512]{1,0:T(8,128)(2,1)}), bf16[2048,512]{1,0:T(8,128)(2,1)}) %all-gather.7.cloned.1.call-update) | async-done | bytes 2097168 | tf_op jit(solution)/shard_map/all_gather | solution.py:114
  76.8 2.9 %convolution_convert_fusion.1 = bf16[512,512]{1,0:T(8,128)(2,1)S(1)} fusion(bf16[2048,512]{1,0:T(8,128)(2,1)} %all-gather.7.cloned.1.call-done, bf16[1,512,2048]{2,1,0:T(8,128)(2,1)S(1)} %copy-done.1, f32[2048]{0:T(1024)} %param.13, f32[512]{0:T(512)} %copy-done.23), kind=kOutput, calls=%fused_computation.13 | convolution fusion | flops 1078198272 | bytes 4728832 | tf_op jit(solution)/shard_map/dot_general | solution.py:123
  79.7 1.5 reshape.236
  81.3 2.3 fusion.4
  83.5 0.1 broadcast_maximum_fusion
  83.6 1.0 fusion.3
  84.6 0.1 exponential_add_fusion
  84.7 1.2 fusion.7
  85.9 0.4 copy.49
  86.3 38.3 %all-gather.11.cloned.1.call-done = bf16[2048,512]{1,0:T(8,128)(2,1)} async-done(((bf16[512,512]{1,0:T(8,128)(2,1)}), bf16[2048,512]{1,0:T(8,128)(2,1)}) %all-gather.11.cloned.1.call-update) | async-done | bytes 2097168 | tf_op jit(solution)/shard_map/all_gather | solution.py:117
  124.6 2.9 %convolution_convert_fusion = bf16[512,512]{1,0:T(8,128)(2,1)S(1)} fusion(bf16[2048,512]{1,0:T(8,128)(2,1)} %all-gather.11.cloned.1.call-done, bf16[1,512,2048]{2,1,0:T(8,128)(2,1)S(1)} %copy-done.1, f32[2048]{0:T(1024)S(1)} %copy-done.28, f32[512]{0:T(512)S(1)} %copy-done.24), kind=kOutput, calls=%fused_computation.12 | convolution fusion | flops 1078198272 | bytes 4728832 | tf_op jit(solution)/shard_map/dot_general | solution.py:123
  127.5 0.8 copy-done.2
  128.3 2.4 collective-permute-start.2
  130.7 39.8 %all-gather.9.cloned.1.call-done = bf16[512,2048]{1,0:T(8,128)(2,1)} async-done(((bf16[512,512]{1,0:T(8,128)(2,1)}), bf16[512,2048]{1,0:T(8,128)(2,1)}) %all-gather.9.cloned.1.call-update) | async-done | bytes 2097168 | tf_op jit(solution)/shard_map/all_gather | solution.py:155
  170.6 4.9 %fusion.29 = f32[512,2048]{1,0:T(8,128)} fusion(bf16[512,2048]{1,0:T(8,128)(2,1)} %all-gather.9.cloned.1.call-done, bf16[64,8,4,128]{3,2,1,0:T(4,128)(2,1)S(1)} %bitcast.76), kind=kOutput, calls=%fused_computation.59 | convolution fusion | flops 1073741824 | bytes 6815744 | tf_op jit(solution)/shard_map/dot_general | solution.py:159
  175.5 0.1 maximum_convert_fusion
  175.8 3.0 %fusion.28 = bf16[512,512]{1,0:T(8,128)(2,1)S(1)} fusion(f32[528,512]{1,0:T(8,128)S(1)} %maximum_convert_fusion, s32[512]{0:T(512)S(1)} %select_reduce_fusion, s32[512]{0:T(512)S(1)} %add_add_fusion, pred[512]{0:T(512)(128)(4,1)S(1)} %copy-done.8, pred[512]{0:T(512)(128)(4,1)S(1)} %copy-done.9, pred[512]{0:T(512)(128)(4,1)S(1)} %copy-done.10, ...), kind=kLoop, calls=%fused_computation.55 | loop fusion | flops 9437184 | bytes 17313792 | tf_op jit(solution)/shard_map/convert_element_type | solution.py:84
  178.8 0.4 fusion.32
  179.2 0.1 fusion.25
  179.3 37.1 %all-gather.13.cloned.1.call-done = bf16[512,2048]{1,0:T(8,128)(2,1)} async-done(((bf16[512,512]{1,0:T(8,128)(2,1)}), bf16[512,2048]{1,0:T(8,128)(2,1)}) %all-gather.13.cloned.1.call-update) | async-done | bytes 2097168 | tf_op jit(solution)/shard_map/all_gather | solution.py:156
  216.4 6.1 %convolution_add_fusion = f32[512,2048]{1,0:T(8,128)} fusion(f32[512,2048]{1,0:T(8,128)} %fusion.29, bf16[512,512]{0,1:T(8,128)(2,1)S(1)} %fusion.25, bf16[512,2048]{1,0:T(8,128)(2,1)} %all-gather.13.cloned.1.call-done), kind=kOutput, calls=%fused_computation.9 | convolution fusion | flops 1074790400 | bytes 11010048 | tf_op jit(solution)/shard_map/dot_general | solution.py:160
  222.5 0.0 reduce-scatter.2.cloned.1.call-update
  222.5 0.7 fusion.43
  223.2 10.3 %reduce-scatter.2.cloned.1.call-done = f32[256,2048]{1,0:T(8,128)} async-done(((f32[512,2048]{1,0:T(8,128)}), f32[256,2048]{1,0:T(8,128)}) %reduce-scatter.2.cloned.1.call-update) | async-done | bytes 2097168 | tf_op jit(solution)/shard_map/reduce_scatter | solution.py:158
  233.5 2.7 %convert_bitcast_fusion = bf16[1,256,2048]{2,1,0:T(8,128)(2,1)} fusion(f32[256,2048]{1,0:T(8,128)} %reduce-scatter.2.cloned.1.call-done), kind=kLoop, calls=%fused_computation.54 | loop fusion | flops 524288 | bytes 3145728 | tf_op jit(solution)/shard_map/broadcast_in_dim | solution.py:165
  (66 shorter events, 0.2 us)
Async XLA Ops:
  7.2 171.7 %copy-start = (bf16[4,256,256]{2,1,0:T(8,128)(2,1)S(1)}, bf16[4,256,256]{2,1,0:T(8,128)(2,1)}, u32[]{:S(2)}) copy-start(bf16[4,256,256]{2,1,0:T(8,128)(2,1)} %param.19) | copy-start | bytes 1572868
  7.2 45.5 %copy-start.26 = (s32[4]{0:T(128)S(1)}, s32[4]{0:T(128)}, u32[]{:S(2)}) copy-start(s32[4]{0:T(128)} %constant.89.clone) | copy-start | bytes 52
  7.2 46.2 %copy-start.25 = (f32[1024]{0:T(1024)S(1)}, f32[1024]{0:T(1024)}, u32[]{:S(2)}) copy-start(f32[1024]{0:T(1024)} %param.20) | copy-start | bytes 12292
  7.2 48.9 %copy-start.27 = (f32[2048]{0:T(1024)S(1)}, f32[2048]{0:T(1024)}, u32[]{:S(2)}) copy-start(f32[2048]{0:T(1024)} %param.13) | copy-start | bytes 24580
  7.2 46.6 %all-gather.15.cloned.1.call-start = ((), (), s32[]{:S(2)}) async-start(), calls=%async_computation.6 | async-start | bytes 3145728 | tf_op jit(solution)/shard_map/all_gather | solution.py:119
  7.9 68.9 %all-gather.7.cloned.1.call-start = ((), (), s32[]{:S(2)}) async-start(), calls=%async_computation.1 | async-start | bytes 2621440 | tf_op jit(solution)/shard_map/all_gather | solution.py:114
  8.7 115.9 %all-gather.11.cloned.1.call-start = ((), (), s32[]{:S(2)}) async-start(), calls=%async_computation.3 | async-start | bytes 2621440 | tf_op jit(solution)/shard_map/all_gather | solution.py:117
  9.4 161.1 %all-gather.9.cloned.1.call-start = ((), (), s32[]{:S(2)}) async-start(), calls=%async_computation.2 | async-start | bytes 2621440 | tf_op jit(solution)/shard_map/all_gather | solution.py:155
  10.0 206.4 %all-gather.13.cloned.1.call-start = ((), (), s32[]{:S(2)}) async-start(), calls=%async_computation.4 | async-start | bytes 2621440 | tf_op jit(solution)/shard_map/all_gather | solution.py:156
  10.6 222.9 %reduce-scatter.2.cloned.1.call-start = ((), (), s32[]{:S(2)}) async-start(), calls=%async_computation.5 | async-start | bytes 6291456 | tf_op jit(solution)/shard_map/reduce_scatter | solution.py:158
  53.8 8.8 %copy-start.1 = (bf16[1,512,2048]{2,1,0:T(8,128)(2,1)S(1)}, bf16[1,512,2048]{2,1,0:T(8,128)(2,1)}, u32[]{:S(2)}) copy-start(bf16[1,512,2048]{2,1,0:T(8,128)(2,1)} %all-gather.15.cloned.1.call-done) | copy-start | bytes 6291460
  53.8 8.8 %copy-start.4 = (bf16[2048,128]{1,0:T(8,128)(2,1)S(1)}, bf16[2048,128]{1,0:T(8,128)(2,1)}, u32[]{:S(2)}) copy-start(bf16[2048,128]{1,0:T(8,128)(2,1)} %all_gather.22) | copy-start | bytes 1572868
  56.1 6.5 %copy-start.23 = (f32[512]{0:T(512)}, f32[512]{0:T(512)S(1)}, u32[]{:S(2)}) copy-start(f32[512]{0:T(512)S(1)} %add_rsqrt_fusion) | copy-start | bytes 6148
  59.1 9.4 %collective-permute-start.1 = (bf16[128,128]{1,0:T(8,128)(2,1)}, bf16[128,128]{1,0:T(8,128)(2,1)}, u32[]{:S(2)}, u32[]{:S(2)}) collective-permute-start(bf16[128,128]{1,0:T(8,128)(2,1)} %slice.86), channel_id=1, source_target_pairs={{0,8},{8,16},{16,24},{1,9},{9,17},{17,25},{2,10},{10,18},{18,26},{... | collective-permute-start | bytes 98312 | tf_op jit(solution)/shard_map/ppermute | solution.py:16
  65.8 4.6 %collective-permute-start = (bf16[128,128]{1,0:T(8,128)(2,1)}, bf16[128,128]{1,0:T(8,128)(2,1)S(1)}, u32[]{:S(2)}, u32[]{:S(2)}) collective-permute-start(bf16[128,128]{1,0:T(8,128)(2,1)} %slice.85), channel_id=1, source_target_pairs={{0,8},{8,16},{16,24},{1,9},{9,17},{17,25},{2,10},{10,18},{18,26},{... | collective-permute-start | bytes 98312 | tf_op jit(solution)/shard_map/ppermute | solution.py:16
  81.2 3.4 %copy-start.5 = (bf16[4,128,2,64]{1,3,2,0:T(8,128)(2,1)S(1)}, bf16[4,128,2,64]{1,3,2,0:T(8,128)(2,1)}, u32[]{:S(2)}) copy-start(bf16[4,128,2,64]{1,3,2,0:T(8,128)(2,1)} %copy.41) | copy-start | bytes 393220
  81.2 3.4 %copy-start.6 = (bf16[4,128,2,64]{1,3,2,0:T(8,128)(2,1)S(1)}, bf16[4,128,2,64]{1,3,2,0:T(8,128)(2,1)}, u32[]{:S(2)}) copy-start(bf16[4,128,2,64]{1,3,2,0:T(8,128)(2,1)} %copy.40) | copy-start | bytes 393220
  84.7 39.9 %copy-start.24 = (f32[512]{0:T(512)S(1)}, f32[512]{0:T(512)}, u32[]{:S(2)}) copy-start(f32[512]{0:T(512)} %copy-done.23) | copy-start | bytes 6148
  84.7 39.9 %copy-start.28 = (f32[2048]{0:T(1024)S(1)}, f32[2048]{0:T(1024)}, u32[]{:S(2)}) copy-start(f32[2048]{0:T(1024)} %param.13) | copy-start | bytes 24580
  127.5 0.8 copy-start.2
  128.3 47.2 %copy-start.3 = (bf16[512,512]{1,0:T(8,128)(2,1)S(1)}, bf16[512,512]{1,0:T(8,128)(2,1)}, u32[]{:S(2)}) copy-start(bf16[512,512]{1,0:T(8,128)(2,1)} %copy-done.2) | copy-start | bytes 1572868
  128.3 47.2 %collective-permute-start.2 = (bf16[16,512]{1,0:T(8,128)(2,1)S(1)}, bf16[16,512]{1,0:T(8,128)(2,1)S(1)}, u32[]{:S(2)}, u32[]{:S(2)}) collective-permute-start(bf16[16,512]{1,0:T(8,128)(2,1)S(1)} %slice.87), channel_id=1, source_target_pairs={{0,8},{8,16},{16,24},{1,9},{9,17},{17,25},{2,10},{10,18},{18,26},{... | collective-permute-start | bytes 49160 | tf_op jit(solution)/shard_map/ppermute | solution.py:16
  170.5 5.1 %copy-start.7 = (pred[512]{0:T(512)(128)(4,1)S(1)}, pred[512]{0:T(512)(128)(4,1)}, u32[]{:S(2)}) copy-start(pred[512]{0:T(512)(128)(4,1)} %get-tuple-element.2) | copy-start | bytes 1540
  170.5 5.1 %copy-start.8 = (pred[512]{0:T(512)(128)(4,1)S(1)}, pred[512]{0:T(512)(128)(4,1)}, u32[]{:S(2)}) copy-start(pred[512]{0:T(512)(128)(4,1)} %get-tuple-element.3) | copy-start | bytes 1540
  170.5 5.1 %copy-start.9 = (pred[512]{0:T(512)(128)(4,1)S(1)}, pred[512]{0:T(512)(128)(4,1)}, u32[]{:S(2)}) copy-start(pred[512]{0:T(512)(128)(4,1)} %get-tuple-element.4) | copy-start | bytes 1540
  170.5 5.1 %copy-start.10 = (pred[512]{0:T(512)(128)(4,1)S(1)}, pred[512]{0:T(512)(128)(4,1)}, u32[]{:S(2)}) copy-start(pred[512]{0:T(512)(128)(4,1)} %get-tuple-element.5) | copy-start | bytes 1540
  170.5 5.1 %copy-start.11 = (pred[512]{0:T(512)(128)(4,1)S(1)}, pred[512]{0:T(512)(128)(4,1)}, u32[]{:S(2)}) copy-start(pred[512]{0:T(512)(128)(4,1)} %get-tuple-element.6) | copy-start | bytes 1540
  170.5 5.2 %copy-start.12 = (pred[512]{0:T(512)(128)(4,1)S(1)}, pred[512]{0:T(512)(128)(4,1)}, u32[]{:S(2)}) copy-start(pred[512]{0:T(512)(128)(4,1)} %get-tuple-element.7) | copy-start | bytes 1540
  170.5 5.2 %copy-start.13 = (pred[512]{0:T(512)(128)(4,1)S(1)}, pred[512]{0:T(512)(128)(4,1)}, u32[]{:S(2)}) copy-start(pred[512]{0:T(512)(128)(4,1)} %get-tuple-element.8) | copy-start | bytes 1540
  170.6 5.2 %copy-start.14 = (pred[512]{0:T(512)(128)(4,1)S(1)}, pred[512]{0:T(512)(128)(4,1)}, u32[]{:S(2)}) copy-start(pred[512]{0:T(512)(128)(4,1)} %get-tuple-element.9) | copy-start | bytes 1540
  170.6 5.2 %copy-start.15 = (pred[512]{0:T(512)(128)(4,1)S(1)}, pred[512]{0:T(512)(128)(4,1)}, u32[]{:S(2)}) copy-start(pred[512]{0:T(512)(128)(4,1)} %get-tuple-element.10) | copy-start | bytes 1540
  170.6 5.2 %copy-start.16 = (pred[512]{0:T(512)(128)(4,1)S(1)}, pred[512]{0:T(512)(128)(4,1)}, u32[]{:S(2)}) copy-start(pred[512]{0:T(512)(128)(4,1)} %get-tuple-element.11) | copy-start | bytes 1540
  170.6 5.2 %copy-start.17 = (pred[512]{0:T(512)(128)(4,1)S(1)}, pred[512]{0:T(512)(128)(4,1)}, u32[]{:S(2)}) copy-start(pred[512]{0:T(512)(128)(4,1)} %get-tuple-element.12) | copy-start | bytes 1540
  170.6 5.2 %copy-start.18 = (pred[512]{0:T(512)(128)(4,1)S(1)}, pred[512]{0:T(512)(128)(4,1)}, u32[]{:S(2)}) copy-start(pred[512]{0:T(512)(128)(4,1)} %get-tuple-element.13) | copy-start | bytes 1540
  170.6 5.2 %copy-start.19 = (pred[512]{0:T(512)(128)(4,1)S(1)}, pred[512]{0:T(512)(128)(4,1)}, u32[]{:S(2)}) copy-start(pred[512]{0:T(512)(128)(4,1)} %get-tuple-element.14) | copy-start | bytes 1540
  170.6 5.2 %copy-start.20 = (pred[512]{0:T(512)(128)(4,1)S(1)}, pred[512]{0:T(512)(128)(4,1)}, u32[]{:S(2)}) copy-start(pred[512]{0:T(512)(128)(4,1)} %get-tuple-element.15) | copy-start | bytes 1540
  170.6 5.2 %copy-start.21 = (pred[512]{0:T(512)(128)(4,1)S(1)}, pred[512]{0:T(512)(128)(4,1)}, u32[]{:S(2)}) copy-start(pred[512]{0:T(512)(128)(4,1)} %get-tuple-element.16) | copy-start | bytes 1540
  170.6 5.2 %copy-start.22 = (pred[512]{0:T(512)(128)(4,1)S(1)}, pred[512]{0:T(512)(128)(4,1)}, u32[]{:S(2)}) copy-start(pred[512]{0:T(512)(128)(4,1)} %get-tuple-element.17) | copy-start | bytes 1540
Sparse Core Ops, SparseCore 0:
  9.6 13.2 all-gather.14
  24.5 52.2 all-gather.6
  78.4 46.1 all-gather.10
  126.0 44.4 all-gather.8
  171.9 44.4 all-gather.12
  222.7 10.8 reduce-scatter.1
where the time goes:
time: 244 us; the launch traced here: 243 us
  waiting for transfers between devices  134 us (55%)
  blocking collectives  41 us (17%)
  matrix products  24.4 us (10%)
  between operations  14.6 us (6%)
  other arithmetic  12.1 us (5%)
  local copies, waits for them, and re-layouts  8.64 us (4%)
  starting transfers between devices  8.09 us (3%)
    all_gather x1, waiting for transfers between devices, local(): lax.all_gather(attn_out_weight, 'sp', axis=1, tiled=True)  39.8 us
    all_gather x1, waiting for transfers between devices, local(): lax.all_gather(pool_in_weight, 'sp', axis=0, tiled=True)  38.3 us
    all_gather x1, waiting for transfers between devices, local(): lax.all_gather(pool_out_weight, 'sp', axis=1, tiled=True)  37.1 us
    all_gather x1, blocking collectives, local(): lax.all_gather(value_matrix, 'sp', axis=0, tiled=True)  23.4 us
    all_gather x1, blocking collectives, local(): lax.all_gather(key_matrix, 'sp', axis=0, tiled=True)  17.6 us
    reduce_scatter x1, waiting for transfers between devices, local(): lax.psum_scatter(jnp.dot(attn_part, half_attn, preferred_element_type=jnp...  10.3 us
    dot_general x4, matrix products, local(): jnp.dot(normed, weight, preferred_element_type=jnp.float32)  9.63 us
    ppermute x3, starting transfers between devices, passed_along(): return lax.ppermute(shard, axis, pairs)  7.87 us
  transfers between devices with their start and end apart: 9, of which 6 were waited for; matrix products, arithmetic and copies ran while one was open for 15% of the time, Pallas kernels for 0%

commit v1 on v0

--- a/solution.py
+++ b/solution.py
@@ -8,6 +8,11 @@
 POOL_CH = 256
 EPSILON = 1e-06
 POOL_SPANS = (2, 4, 8, 16)
+
+
+def stack_and_merge(block, axis, dim):
+    blocks = lax.all_gather(block, axis)
+    return jnp.concatenate(blocks, axis=dim)
 
 
 def passed_along(shard, axis, by):
@@ -153,7 +158,7 @@
     pool_part = pool_branch(pool_rows, pool_tail, mixing, scales, tp_index * groups_dev, first_pos)
     half_attn, half_pool = (
         lax.all_gather(attn_out_weight, "sp", axis=1, tiled=True),
-        lax.all_gather(pool_out_weight, "sp", axis=1, tiled=True),
+        stack_and_merge(pool_out_weight, "sp", 1),
     )
     result = lax.psum_scatter(
         jnp.dot(attn_part, half_attn, preferred_element_type=jnp.float32)

time: 244 us -> 247 us (1.012)
  waiting for transfers between devices: 134 us -> 138 us
  local copies, waits for them, and re-layouts: 8.64 us -> 12.1 us
  matrix products: 24.4 us -> 21.7 us
    all_gather x1, waiting for transfers between devices: 37.1 us -> 40.9 us  [stack_and_merge(): blocks = lax.all_gather(block, axis)]
    reshape x0 -> x1, local copies, waits for them, and re-layouts: none -> 2.79 us  [stack_and_merge(): return jnp.concatenate(blocks, axis=dim)]
    dot_general x1, matrix products: 6.08 us -> 3.33 us  [local(): jnp.dot(pool_part, half_pool, preferred_element_type=jnp.float32)]
  transfers between devices with their start and end apart: 9 -> 9, of which waited for: 6 -> 6; matrix products, arithmetic and copies ran while one was open for 15% -> 14% of each run, Pallas kernels for 0% -> 0%
where the time goes in v1:
time: 247 us
  waiting for transfers between devices  138 us (56%)
  blocking collectives  41 us (17%)
  matrix products  21.7 us (9%)
  between operations  14.7 us (6%)
  local copies, waits for them, and re-layouts  12.1 us (5%)
  other arithmetic  11.9 us (5%)
  starting transfers between devices  7.95 us (3%)
    all_gather x1, waiting for transfers between devices, stack_and_merge(): blocks = lax.all_gather(block, axis)  40.9 us
    all_gather x1, waiting for transfers between devices, local(): lax.all_gather(attn_out_weight, 'sp', axis=1, tiled=True)  40 us
    all_gather x1, waiting for transfers between devices, local(): lax.all_gather(pool_in_weight, 'sp', axis=0, tiled=True)  38.3 us
    all_gather x1, blocking collectives, local(): lax.all_gather(value_matrix, 'sp', axis=0, tiled=True)  23.4 us
    all_gather x1, blocking collectives, local(): lax.all_gather(key_matrix, 'sp', axis=0, tiled=True)  17.6 us
    reduce_scatter x1, waiting for transfers between devices, local(): lax.psum_scatter(jnp.dot(attn_part, half_attn, preferred_element_type=jnp...  10.3 us
    dot_general x4, matrix products, local(): jnp.dot(normed, weight, preferred_element_type=jnp.float32)  9.65 us
    ppermute x3, starting transfers between devices, passed_along(): return lax.ppermute(shard, axis, pairs)  7.72 us
  transfers between devices with their start and end apart: 9, of which 6 were waited for; matrix products, arithmetic and copies ran while one was open for 14% of the time, Pallas kernels for 0%

profile of v1, /device:TPU:0, one launch (start us, length us, event | category | flops | bytes accessed | tf_op | source)
XLA Modules:
  0.0 246.9 jit_solution(6794155017344855070)
XLA Ops:
  7.2 0.0 all-gather.14.cloned.1.call-start
  7.3 0.7 all-gather.14.cloned.1.call-update
  7.9 0.0 all-gather.8.cloned.1.call-start
  8.0 0.7 all-gather.8.cloned.1.call-update
  8.7 0.0 all-gather.12.cloned.1.call-start
  8.7 0.7 all-gather.12.cloned.1.call-update
  9.4 0.0 all-gather.10.cloned.1.call-start
  9.5 0.5 all-gather.10.cloned.1.call-update
  10.0 0.0 all-gather.16.cloned.1.call-start
  10.1 0.5 all-gather.16.cloned.1.call-update
  10.6 0.0 reduce-scatter.2.cloned.1.call-start
  10.7 0.1 iota_add_fusion
  10.7 0.1 broadcast_compare_fusion
  10.8 17.6 %all_gather.26 = bf16[2048,128]{1,0:T(8,128)(2,1)S(1)} all-gather(bf16[512,128]{1,0:T(8,128)(2,1)} %param.15), channel_id=1, replica_groups=mesh['sp'=4,'fs'=4,'tp'=2] {'sp'}, dimensions={0}, use_global_device_ids=true | all-gather | bytes 655360 | tf_op jit(solution)/shard_map/all_gather | solution.py:120
  28.4 0.7 dynamic_slice.9
  29.1 0.1 max.26
  29.2 23.4 %all_gather.25 = bf16[2048,128]{1,0:T(8,128)(2,1)} all-gather(bf16[512,128]{1,0:T(8,128)(2,1)} %param.16), channel_id=1, replica_groups=mesh['sp'=4,'fs'=4,'tp'=2] {'sp'}, dimensions={0}, use_global_device_ids=true | all-gather | bytes 655360 | tf_op jit(solution)/shard_map/all_gather | solution.py:121
  52.6 0.1 select_reduce_fusion
  52.7 0.6 broadcast_compare_fusion.15
  53.4 0.1 dynamic_slice.11
  53.5 0.6 mul.74
  54.1 0.3 fusion.35
  54.4 0.0 all-gather.14.cloned.1.call-done
  54.5 2.2 fusion
  56.7 2.4 convolution_convert_fusion.2
  59.1 0.6 slice.86
  59.7 3.5 %collective-permute-start.1 = (bf16[128,128]{1,0:T(8,128)(2,1)}, bf16[128,128]{1,0:T(8,128)(2,1)}, u32[]{:S(2)}, u32[]{:S(2)}) collective-permute-start(bf16[128,128]{1,0:T(8,128)(2,1)} %slice.86), channel_id=1, source_target_pairs={{0,8},{8,16},{16,24},{1,9},{9,17},{17,25},{2,10},{10,18},{18,26},{... | collective-permute-start | bytes 98312 | tf_op jit(solution)/shard_map/ppermute | solution.py:21
  63.2 1.5 convolution_convert_fusion.3
  64.7 0.1 reshape.247
  64.8 0.6 slice.85
  65.4 0.1 reshape.245
  65.6 0.8 copy.61
  66.4 2.0 collective-permute-start
  68.4 0.8 copy.57
  69.2 0.8 pad_maximum_fusion
  69.9 0.1 reshape.246
  70.1 0.8 copy.60
  70.9 0.1 collective-permute-done
  71.0 0.1 reshape.244
  71.1 0.8 copy.56
  71.9 4.9 %all-gather.8.cloned.1.call-done = bf16[2048,512]{1,0:T(8,128)(2,1)} async-done(((bf16[512,512]{1,0:T(8,128)(2,1)}), bf16[2048,512]{1,0:T(8,128)(2,1)}) %all-gather.8.cloned.1.call-update) | async-done | bytes 2097168 | tf_op jit(solution)/shard_map/all_gather | solution.py:119
  76.8 2.9 %convolution_convert_fusion.1 = bf16[512,512]{1,0:T(8,128)(2,1)S(1)} fusion(bf16[2048,512]{1,0:T(8,128)(2,1)} %all-gather.8.cloned.1.call-done, bf16[1,512,2048]{2,1,0:T(8,128)(2,1)S(1)} %copy-done.2, f32[2048]{0:T(1024)} %param.13, f32[512]{0:T(512)} %copy-done.24), kind=kOutput, calls=%fused_computation.14 | convolution fusion | flops 1078198272 | bytes 4728832 | tf_op jit(solution)/shard_map/dot_general | solution.py:128
  79.7 1.5 reshape.248
  81.3 2.3 fusion.4
  83.5 0.1 broadcast_maximum_fusion
  83.6 1.0 fusion.3
  84.6 0.1 exponential_add_fusion
  84.7 1.2 fusion.8
  85.9 0.4 copy.65
  86.3 38.3 %all-gather.12.cloned.1.call-done = bf16[2048,512]{1,0:T(8,128)(2,1)} async-done(((bf16[512,512]{1,0:T(8,128)(2,1)}), bf16[2048,512]{1,0:T(8,128)(2,1)}) %all-gather.12.cloned.1.call-update) | async-done | bytes 2097168 | tf_op jit(solution)/shard_map/all_gather | solution.py:122
  124.6 2.9 %convolution_convert_fusion = bf16[512,512]{1,0:T(8,128)(2,1)S(1)} fusion(bf16[2048,512]{1,0:T(8,128)(2,1)} %all-gather.12.cloned.1.call-done, bf16[1,512,2048]{2,1,0:T(8,128)(2,1)S(1)} %copy-done.2, f32[2048]{0:T(1024)S(1)} %copy-done.29, f32[512]{0:T(512)S(1)} %copy-done.25), kind=kOutput, calls=%fused_computation.13 | convolution fusion | flops 1078198272 | bytes 4728832 | tf_op jit(solution)/shard_map/dot_general | solution.py:128
  127.5 0.8 copy-done.3
  128.3 2.2 collective-permute-start.2
  130.6 40.0 %all-gather.10.cloned.1.call-done = bf16[512,2048]{1,0:T(8,128)(2,1)} async-done(((bf16[512,512]{1,0:T(8,128)(2,1)}), bf16[512,2048]{1,0:T(8,128)(2,1)}) %all-gather.10.cloned.1.call-update) | async-done | bytes 2097168 | tf_op jit(solution)/shard_map/all_gather | solution.py:160
  170.5 4.8 %fusion.29 = f32[512,2048]{1,0:T(8,128)} fusion(bf16[512,2048]{1,0:T(8,128)(2,1)} %all-gather.10.cloned.1.call-done, bf16[64,8,4,128]{3,2,1,0:T(4,128)(2,1)S(1)} %bitcast.78), kind=kOutput, calls=%fused_computation.59 | convolution fusion | flops 1073741824 | bytes 6815744 | tf_op jit(solution)/shard_map/dot_general | solution.py:164
  175.5 40.9 %all-gather.16.cloned.1.call-done = bf16[2048,512]{1,0:T(8,128)(2,1)} async-done(((bf16[512,512]{1,0:T(8,128)(2,1)}), bf16[2048,512]{1,0:T(8,128)(2,1)}) %all-gather.16.cloned.1.call-update) | async-done | bytes 2097168 | tf_op jit(solution)/shard_map/all_gather | solution.py:14
  216.4 2.8 %copy.68 = bf16[512,4,512]{0,2,1:T(8,128)(2,1)S(1)} copy(bf16[512,4,512]{2,0,1:T(8,128)(2,1)} %bitcast.77) | data formatting | bytes 4194304 | tf_op jit(solution)/shard_map/reshape | solution.py:15
  219.2 0.1 maximum_convert_fusion
  219.6 3.0 %fusion.28 = bf16[512,512]{1,0:T(8,128)(2,1)S(1)} fusion(f32[528,512]{1,0:T(8,128)S(1)} %maximum_convert_fusion, s32[512]{0:T(512)S(1)} %select_reduce_fusion, s32[512]{0:T(512)S(1)} %add_add_fusion, pred[512]{0:T(512)(128)(4,1)S(1)} %copy-done.8, pred[512]{0:T(512)(128)(4,1)S(1)} %copy-done.9, pred[512]{0:T(512)(128)(4,1)S(1)} %copy-done.10, ...), kind=kLoop, calls=%fused_computation.55 | loop fusion | flops 9437184 | bytes 17313792 | tf_op jit(solution)/shard_map/convert_element_type | solution.py:89
  222.6 0.4 fusion.6
  223.0 3.3 %convolution_add_fusion = f32[512,2048]{1,0:T(8,128)} fusion(f32[512,2048]{1,0:T(8,128)S(1)} %copy-done.1, bf16[512,512]{0,1:T(8,128)(2,1)S(1)} %bitcast.80, bf16[512,2048]{0,1:T(8,128)(2,1)S(1)} %bitcast.76), kind=kOutput, calls=%fused_computation.9 | convolution fusion | flops 1074790400 | bytes 11010048 | tf_op jit(solution)/shard_map/dot_general | solution.py:165
  226.3 0.7 fusion.42
  227.0 10.3 %reduce-scatter.2.cloned.1.call-done = f32[256,2048]{1,0:T(8,128)} async-done(((f32[512,2048]{1,0:T(8,128)}), f32[256,2048]{1,0:T(8,128)}) %reduce-scatter.2.cloned.1.call-update) | async-done | bytes 2097168 | tf_op jit(solution)/shard_map/reduce_scatter | solution.py:163
  237.3 2.7 %convert_bitcast_fusion = bf16[1,256,2048]{2,1,0:T(8,128)(2,1)} fusion(f32[256,2048]{1,0:T(8,128)} %reduce-scatter.2.cloned.1.call-done), kind=kLoop, calls=%fused_computation.54 | loop fusion | flops 524288 | bytes 3145728 | tf_op jit(solution)/shard_map/broadcast_in_dim | solution.py:170
  (69 shorter events, 0.2 us)
Async XLA Ops:
  7.2 215.4 %copy-start = (bf16[4,256,256]{2,1,0:T(8,128)(2,1)S(1)}, bf16[4,256,256]{2,1,0:T(8,128)(2,1)}, u32[]{:S(2)}) copy-start(bf16[4,256,256]{2,1,0:T(8,128)(2,1)} %param.19) | copy-start | bytes 1572868
  7.2 45.5 %copy-start.27 = (s32[4]{0:T(128)S(1)}, s32[4]{0:T(128)}, u32[]{:S(2)}) copy-start(s32[4]{0:T(128)} %constant.89.clone) | copy-start | bytes 52
  7.2 46.2 %copy-start.26 = (f32[1024]{0:T(1024)S(1)}, f32[1024]{0:T(1024)}, u32[]{:S(2)}) copy-start(f32[1024]{0:T(1024)} %param.20) | copy-start | bytes 12292
  7.2 49.5 %copy-start.28 = (f32[2048]{0:T(1024)S(1)}, f32[2048]{0:T(1024)}, u32[]{:S(2)}) copy-start(f32[2048]{0:T(1024)} %param.13) | copy-start | bytes 24580
  7.2 47.2 %all-gather.14.cloned.1.call-start = ((), (), s32[]{:S(2)}) async-start(), calls=%async_computation.5 | async-start | bytes 3145728 | tf_op jit(solution)/shard_map/all_gather | solution.py:124
  7.9 68.9 %all-gather.8.cloned.1.call-start = ((), (), s32[]{:S(2)}) async-start(), calls=%async_computation.1 | async-start | bytes 2621440 | tf_op jit(solution)/shard_map/all_gather | solution.py:119
  8.7 115.9 %all-gather.12.cloned.1.call-start = ((), (), s32[]{:S(2)}) async-start(), calls=%async_computation.3 | async-start | bytes 2621440 | tf_op jit(solution)/shard_map/all_gather | solution.py:122
  9.4 161.1 %all-gather.10.cloned.1.call-start = ((), (), s32[]{:S(2)}) async-start(), calls=%async_computation.2 | async-start | bytes 2621440 | tf_op jit(solution)/shard_map/all_gather | solution.py:160
  10.0 206.4 %all-gather.16.cloned.1.call-start = ((), (), s32[]{:S(2)}) async-start(), calls=%async_computation.6 | async-start | bytes 2621440 | tf_op jit(solution)/shard_map/all_gather | solution.py:14
  10.6 226.7 %reduce-scatter.2.cloned.1.call-start = ((), (), s32[]{:S(2)}) async-start(), calls=%async_computation.4 | async-start | bytes 6291456 | tf_op jit(solution)/shard_map/reduce_scatter | solution.py:163
  54.4 8.8 %copy-start.2 = (bf16[1,512,2048]{2,1,0:T(8,128)(2,1)S(1)}, bf16[1,512,2048]{2,1,0:T(8,128)(2,1)}, u32[]{:S(2)}) copy-start(bf16[1,512,2048]{2,1,0:T(8,128)(2,1)} %all-gather.14.cloned.1.call-done) | copy-start | bytes 6291460
  54.4 8.8 %copy-start.5 = (bf16[2048,128]{1,0:T(8,128)(2,1)S(1)}, bf16[2048,128]{1,0:T(8,128)(2,1)}, u32[]{:S(2)}) copy-start(bf16[2048,128]{1,0:T(8,128)(2,1)} %all_gather.25) | copy-start | bytes 1572868
  56.7 6.5 %copy-start.24 = (f32[512]{0:T(512)}, f32[512]{0:T(512)S(1)}, u32[]{:S(2)}) copy-start(f32[512]{0:T(512)S(1)} %add_rsqrt_fusion) | copy-start | bytes 6148
  59.7 9.5 %collective-permute-start.1 = (bf16[128,128]{1,0:T(8,128)(2,1)}, bf16[128,128]{1,0:T(8,128)(2,1)}, u32[]{:S(2)}, u32[]{:S(2)}) collective-permute-start(bf16[128,128]{1,0:T(8,128)(2,1)} %slice.86), channel_id=1, source_target_pairs={{0,8},{8,16},{16,24},{1,9},{9,17},{17,25},{2,10},{10,18},{18,26},{... | collective-permute-start | bytes 98312 | tf_op jit(solution)/shard_map/ppermute | solution.py:21
  66.4 4.6 %collective-permute-start = (bf16[128,128]{1,0:T(8,128)(2,1)}, bf16[128,128]{1,0:T(8,128)(2,1)S(1)}, u32[]{:S(2)}, u32[]{:S(2)}) collective-permute-start(bf16[128,128]{1,0:T(8,128)(2,1)} %slice.85), channel_id=1, source_target_pairs={{0,8},{8,16},{16,24},{1,9},{9,17},{17,25},{2,10},{10,18},{18,26},{... | collective-permute-start | bytes 98312 | tf_op jit(solution)/shard_map/ppermute | solution.py:21
  81.2 3.4 %copy-start.6 = (bf16[4,128,2,64]{1,3,2,0:T(8,128)(2,1)S(1)}, bf16[4,128,2,64]{1,3,2,0:T(8,128)(2,1)}, u32[]{:S(2)}) copy-start(bf16[4,128,2,64]{1,3,2,0:T(8,128)(2,1)} %copy.57) | copy-start | bytes 393220
  81.2 3.4 %copy-start.7 = (bf16[4,128,2,64]{1,3,2,0:T(8,128)(2,1)S(1)}, bf16[4,128,2,64]{1,3,2,0:T(8,128)(2,1)}, u32[]{:S(2)}) copy-start(bf16[4,128,2,64]{1,3,2,0:T(8,128)(2,1)} %copy.56) | copy-start | bytes 393220
  84.7 39.9 %copy-start.25 = (f32[512]{0:T(512)S(1)}, f32[512]{0:T(512)}, u32[]{:S(2)}) copy-start(f32[512]{0:T(512)} %copy-done.24) | copy-start | bytes 6148
  84.7 39.9 %copy-start.29 = (f32[2048]{0:T(1024)S(1)}, f32[2048]{0:T(1024)}, u32[]{:S(2)}) copy-start(f32[2048]{0:T(1024)} %param.13) | copy-start | bytes 24580
  127.5 0.8 copy-start.3
  128.3 90.9 %collective-permute-start.2 = (bf16[16,512]{1,0:T(8,128)(2,1)S(1)}, bf16[16,512]{1,0:T(8,128)(2,1)S(1)}, u32[]{:S(2)}, u32[]{:S(2)}) collective-permute-start(bf16[16,512]{1,0:T(8,128)(2,1)S(1)} %slice.87), channel_id=1, source_target_pairs={{0,8},{8,16},{16,24},{1,9},{9,17},{17,25},{2,10},{10,18},{18,26},{... | collective-permute-start | bytes 49160 | tf_op jit(solution)/shard_map/ppermute | solution.py:21
  175.4 43.9 %copy-start.4 = (bf16[512,512]{1,0:T(8,128)(2,1)S(1)}, bf16[512,512]{1,0:T(8,128)(2,1)}, u32[]{:S(2)}) copy-start(bf16[512,512]{1,0:T(8,128)(2,1)} %copy-done.3) | copy-start | bytes 1572868
  175.4 44.0 %copy-start.8 = (pred[512]{0:T(512)(128)(4,1)S(1)}, pred[512]{0:T(512)(128)(4,1)}, u32[]{:S(2)}) copy-start(pred[512]{0:T(512)(128)(4,1)} %get-tuple-element.3) | copy-start | bytes 1540
  175.4 44.0 %copy-start.9 = (pred[512]{0:T(512)(128)(4,1)S(1)}, pred[512]{0:T(512)(128)(4,1)}, u32[]{:S(2)}) copy-start(pred[512]{0:T(512)(128)(4,1)} %get-tuple-element.4) | copy-start | bytes 1540
  175.4 44.0 %copy-start.10 = (pred[512]{0:T(512)(128)(4,1)S(1)}, pred[512]{0:T(512)(128)(4,1)}, u32[]{:S(2)}) copy-start(pred[512]{0:T(512)(128)(4,1)} %get-tuple-element.5) | copy-start | bytes 1540
  175.4 44.0 %copy-start.11 = (pred[512]{0:T(512)(128)(4,1)S(1)}, pred[512]{0:T(512)(128)(4,1)}, u32[]{:S(2)}) copy-start(pred[512]{0:T(512)(128)(4,1)} %get-tuple-element.6) | copy-start | bytes 1540
  175.4 44.0 %copy-start.12 = (pred[512]{0:T(512)(128)(4,1)S(1)}, pred[512]{0:T(512)(128)(4,1)}, u32[]{:S(2)}) copy-start(pred[512]{0:T(512)(128)(4,1)} %get-tuple-element.7) | copy-start | bytes 1540
  175.4 44.0 %copy-start.13 = (pred[512]{0:T(512)(128)(4,1)S(1)}, pred[512]{0:T(512)(128)(4,1)}, u32[]{:S(2)}) copy-start(pred[512]{0:T(512)(128)(4,1)} %get-tuple-element.8) | copy-start | bytes 1540
  175.4 44.0 %copy-start.14 = (pred[512]{0:T(512)(128)(4,1)S(1)}, pred[512]{0:T(512)(128)(4,1)}, u32[]{:S(2)}) copy-start(pred[512]{0:T(512)(128)(4,1)} %get-tuple-element.9) | copy-start | bytes 1540
  175.4 44.0 %copy-start.15 = (pred[512]{0:T(512)(128)(4,1)S(1)}, pred[512]{0:T(512)(128)(4,1)}, u32[]{:S(2)}) copy-start(pred[512]{0:T(512)(128)(4,1)} %get-tuple-element.10) | copy-start | bytes 1540
  175.4 44.0 %copy-start.16 = (pred[512]{0:T(512)(128)(4,1)S(1)}, pred[512]{0:T(512)(128)(4,1)}, u32[]{:S(2)}) copy-start(pred[512]{0:T(512)(128)(4,1)} %get-tuple-element.11) | copy-start | bytes 1540
  175.4 44.0 %copy-start.17 = (pred[512]{0:T(512)(128)(4,1)S(1)}, pred[512]{0:T(512)(128)(4,1)}, u32[]{:S(2)}) copy-start(pred[512]{0:T(512)(128)(4,1)} %get-tuple-element.12) | copy-start | bytes 1540
  175.4 44.0 %copy-start.18 = (pred[512]{0:T(512)(128)(4,1)S(1)}, pred[512]{0:T(512)(128)(4,1)}, u32[]{:S(2)}) copy-start(pred[512]{0:T(512)(128)(4,1)} %get-tuple-element.13) | copy-start | bytes 1540
  175.5 44.0 %copy-start.19 = (pred[512]{0:T(512)(128)(4,1)S(1)}, pred[512]{0:T(512)(128)(4,1)}, u32[]{:S(2)}) copy-start(pred[512]{0:T(512)(128)(4,1)} %get-tuple-element.14) | copy-start | bytes 1540
  175.5 44.0 %copy-start.20 = (pred[512]{0:T(512)(128)(4,1)S(1)}, pred[512]{0:T(512)(128)(4,1)}, u32[]{:S(2)}) copy-start(pred[512]{0:T(512)(128)(4,1)} %get-tuple-element.15) | copy-start | bytes 1540
  175.5 44.0 %copy-start.21 = (pred[512]{0:T(512)(128)(4,1)S(1)}, pred[512]{0:T(512)(128)(4,1)}, u32[]{:S(2)}) copy-start(pred[512]{0:T(512)(128)(4,1)} %get-tuple-element.16) | copy-start | bytes 1540
  175.5 44.0 %copy-start.22 = (pred[512]{0:T(512)(128)(4,1)S(1)}, pred[512]{0:T(512)(128)(4,1)}, u32[]{:S(2)}) copy-start(pred[512]{0:T(512)(128)(4,1)} %get-tuple-element.17) | copy-start | bytes 1540
  219.5 3.0 %copy-start.23 = (f32[2,256]{1,0:T(2,128)S(1)}, f32[2,256]{1,0:T(2,128)}, u32[]{:S(2)}) copy-start(f32[2,256]{1,0:T(2,128)} %mul.74) | copy-start | bytes 6148
  219.5 3.4 %copy-start.1 = (f32[512,2048]{1,0:T(8,128)S(1)}, f32[512,2048]{1,0:T(8,128)}, u32[]{:S(2)}) copy-start(f32[512,2048]{1,0:T(8,128)} %fusion.29) | copy-start | bytes 12582916
Sparse Core Ops, SparseCore 0:
  9.6 13.2 all-gather.13
  24.5 52.2 all-gather.7
  78.4 46.1 all-gather.11
  126.0 44.4 all-gather.9
  171.9 44.4 all-gather.15
  226.5 10.8 reduce-scatter.1
